TPU v7x, 32 devices: a whole 2x2x4 slice. The times are simulated.
32 devices in a mesh: sp: 8 (over z, x), tp: 4 (over y, core).
Axes of the slice: x: 2, y: 2, z: 4, core: 2. Of those that a mesh axis runs over, the one named last changes fastest.
Arguments:
- residual: bfloat16 [2048, 2048], P('sp', 'tp'), may hold values from -48 to 48
- queries: bfloat16 [2048, 1024], P('sp', 'tp'), may hold values from -6 to 6
- key_rows: bfloat16 [2048, 512], P('sp', 'tp'), may hold values from -6 to 6
- value_rows: bfloat16 [2048, 512], P('sp', 'tp'), may hold values from -6 to 6
- break_shift: bfloat16 [4, 2048], P('tp', 'sp'), may hold values from -20 to 0
- head_gain: float32 [1024], P('tp'), may hold values from 0.1 to 1.9
- out_weight: bfloat16 [1024, 2048], P('tp'), may hold values from -0.1875 to 0.1875
- mlp_gain: float32 [2048], replicated, may hold values from 0.1 to 1.9
- up_weight: bfloat16 [2048, 8192], P('sp', 'tp'), may hold values from -0.125 to 0.125
- down_weight: bfloat16 [8192, 2048], P('tp', 'sp'), may hold values from -0.0625 to 0.0625
Outputs:
- layer_out: bfloat16 [2048, 2048], P('sp', 'tp')
All inputs are finite; a program needn't handle non-finite values.
Results may differ from a plain program's by a relative error of at most 0.013.
Values may be sent and summed in bfloat16 or wider, within the bound.
A program may use at most 128 MiB of HBM per device.

v0:
```python
import jax
import jax.numpy as jnp
from jax import lax
from jax.sharding import PartitionSpec as P

HEAD_DIM = 128
eps = 1e-06


def stick_attention(queries, key_all, value_all, shift_all, first_pos, key_block):
    token_count = queries.shape[0]
    kv_local = key_all.shape[1] // HEAD_DIM
    query_local = queries.shape[1] // HEAD_DIM
    group_size = query_local // kv_local
    stacked = queries.reshape(token_count, kv_local, group_size, HEAD_DIM).transpose(1, 2, 0, 3)
    stacked = stacked.reshape(kv_local, group_size * token_count, HEAD_DIM)
    query_pos = first_pos + lax.iota(jnp.int32, group_size * token_count) % token_count
    score_scale = HEAD_DIM ** (-0.5)
    block_count = (first_pos + token_count - 1 + key_block - 1) // key_block

    def one_block(turn_index, state_pair):
        running, broken_after = state_pair
        offset = (block_count - 1 - turn_index) * key_block
        key_block_rows = lax.dynamic_slice_in_dim(key_all, offset, key_block, 0).reshape(
            key_block, kv_local, HEAD_DIM
        )
        value_block_rows = lax.dynamic_slice_in_dim(value_all, offset, key_block, 0).reshape(
            key_block, kv_local, HEAD_DIM
        )
        shift_block = lax.dynamic_slice_in_dim(shift_all, offset, key_block, 1).astype(jnp.float32)
        scores = jnp.einsum(
            "grd,kgd->grk", stacked, key_block_rows, preferred_element_type=jnp.float32
        )
        scores = scores * score_scale + shift_block[:, None, :]
        key_pos = offset + lax.iota(jnp.int32, key_block)
        visible = key_pos[None, None, :] < query_pos[None, :, None]
        broken = jnp.where(visible, jax.nn.log_sigmoid(-scores), 0.0)
        later = lax.cumsum(broken, axis=2, reverse=True) - broken + broken_after[:, :, None]
        weights = jnp.where(visible, jnp.exp(jax.nn.log_sigmoid(scores) + later), 0.0).astype(
            jnp.bfloat16
        )
        running = running + jnp.einsum(
            "grk,kgd->grd", weights, value_block_rows, preferred_element_type=jnp.float32
        )
        return (running, broken_after + jnp.sum(broken, axis=2))

    start_pair = (
        jnp.zeros((kv_local, group_size * token_count, HEAD_DIM), jnp.float32),
        jnp.zeros((kv_local, group_size * token_count), jnp.float32),
    )
    running, broken_after = lax.fori_loop(0, block_count, one_block, start_pair)
    running = running.reshape(kv_local, group_size, token_count, HEAD_DIM).transpose(2, 0, 1, 3)
    return running.reshape(token_count, query_local, HEAD_DIM)


def body(
    residual,
    queries,
    key_rows,
    value_rows,
    break_shift,
    head_gain,
    out_weight,
    mlp_gain,
    up_weight,
    down_weight,
):
    token_count = queries.shape[0]
    first_pos = lax.axis_index("sp") * token_count
    key_all, value_all, shift_all = (
        lax.all_gather(key_rows, "sp", axis=0, tiled=True),
        lax.all_gather(value_rows, "sp", axis=0, tiled=True),
        lax.all_gather(break_shift, "sp", axis=1, tiled=True),
    )
    key_block = min(2048, key_all.shape[0])
    mixed = stick_attention(queries, key_all, value_all, shift_all, first_pos, key_block)
    power = jnp.mean(mixed * mixed, axis=2, keepdims=True)
    attended = (mixed * lax.rsqrt(power + eps) * head_gain.reshape(-1, HEAD_DIM)).astype(
        jnp.bfloat16
    )
    attended = attended.reshape(token_count, -1)
    partial_value = jnp.dot(attended, out_weight, preferred_element_type=jnp.float32)
    column_count = residual.shape[1]
    column_start = lax.axis_index("tp") * column_count
    own_part = lax.dynamic_slice_in_dim(
        partial_value, column_start, column_count, 1
    ) + residual.astype(jnp.float32)
    partial_value = lax.dynamic_update_slice_in_dim(partial_value, own_part, column_start, 1)
    hidden_whole = lax.psum(partial_value, "tp").astype(jnp.bfloat16)
    widened = hidden_whole.astype(jnp.float32)
    inverse = lax.rsqrt(jnp.mean(widened * widened, axis=1, keepdims=True) + eps)
    mlp_in = (widened * inverse * mlp_gain).astype(jnp.bfloat16)
    hidden_state = lax.dynamic_slice_in_dim(hidden_whole, column_start, column_count, 1)
    lifted = jnp.dot(
        mlp_in,
        lax.all_gather(up_weight, "sp", axis=0, tiled=True),
        preferred_element_type=jnp.float32,
    )
    activated = jnp.square(jax.nn.relu(lifted)).astype(jnp.bfloat16)
    expanded = jnp.dot(
        activated,
        lax.all_gather(down_weight, "sp", axis=1, tiled=True),
        preferred_element_type=jnp.float32,
    )
    mlp_total = lax.psum_scatter(
        expanded.astype(jnp.bfloat16), "tp", scatter_dimension=1, tiled=True
    ).astype(jnp.float32)
    return (hidden_state.astype(jnp.float32) + mlp_total).astype(jnp.bfloat16)


def solution(mesh):
    in_specs = (
        P("sp", "tp"),
        P("sp", "tp"),
        P("sp", "tp"),
        P("sp", "tp"),
        P("tp", "sp"),
        P("tp"),
        P("tp", None),
        P(),
        P("sp", "tp"),
        P("tp", "sp"),
    )
    out_specs = P("sp", "tp")
    return jax.shard_map(body, mesh=mesh, in_specs=in_specs, out_specs=out_specs, check_vma=False)
```

profile of v0, /device:TPU:0, one launch (start us, length us, event | category | flops | bytes accessed | tf_op | source)
XLA Modules:
  0.0 312.5 jit_solution(17928566602720874883)
XLA Ops:
  6.5 0.0 copy-start
  6.5 0.0 all-gather.3.cloned.1.call-start
  6.5 0.7 all-gather.3.cloned.1.call-update
  7.3 0.0 all-gather.5.cloned.1.call-start
  7.3 0.7 all-gather.5.cloned.1.call-update
  8.0 0.0 reduce-scatter.2.cloned.1.call-start
  8.1 35.3 %all_gather.15 = bf16[2048,128]{1,0:T(8,128)(2,1)S(1)} all-gather(bf16[256,128]{1,0:T(8,128)(2,1)} %param.14), channel_id=1, replica_groups=mesh['sp'=8,'tp'=4] {'sp'}, dimensions={0}, use_global_device_ids=true | all-gather | bytes 589824 | tf_op jit(solution)/shard_map/all_gather | solution.py:71
  43.4 33.5 %all_gather.17 = bf16[2048,128]{1,0:T(8,128)(2,1)S(1)} all-gather(bf16[256,128]{1,0:T(8,128)(2,1)} %param.15), channel_id=1, replica_groups=mesh['sp'=8,'tp'=4] {'sp'}, dimensions={0}, use_global_device_ids=true | all-gather | bytes 589824 | tf_op jit(solution)/shard_map/all_gather | solution.py:72
  76.9 0.9 reshape.144
  77.9 22.0 %all_gather.16 = bf16[1,2048]{1,0:T(2,128)(2,1)S(1)} all-gather(bf16[1,256]{1,0:T(2,128)(2,1)} %param.16), channel_id=1, replica_groups=mesh['sp'=8,'tp'=4] {'sp'}, dimensions={1}, use_global_device_ids=true | all-gather | bytes 4608 | tf_op jit(solution)/shard_map/all_gather | solution.py:73
  99.9 0.0 copy-start.3
  99.9 48.2 %while.15 = (s32[]{:T(128)}, f32[1,512,128]{2,1,0:T(8,128)S(1)}, f32[1,512]{1,0:T(1,128)S(1)}, s32[]{:T(128)}, s32[]{:T(128)}, /*index=5*/bf16[1,512,128]{2,1,0:...) while((s32[]{:T(128)}, f32[1,512,128]{2,1,0:T(8,128)S(1)}, ...), condition=%wide.region_4.5_spmd.clone, body=%wide.region_0.4_spmd.clone.sunk | while | flops 709041152 | bytes 81762496 | solution.py:51
  100.0 2.6 fusion.64
  102.6 5.0 %fusion.66 = (f32[512]{0:T(512)S(1)}, f32[64,8,16,128]{3,1,2,0:T(8,128)S(1)}) fusion(f32[2048]{0:T(1024)S(1)} %bitcast.98, f32[512,2048]{1,0:T(8,128)} %fusion.64, s32[512]{0:T(512)S(1)} %fusion.65, s32[2048]{0:T(1024)S(1)} %iota_add_fusion.2), kind=kLoop, calls=%fused_computation.30.clone.1 | loop fusion | flops 12582400 | bytes 8409088 | tf_op jit(solution)/shard_map/while/body/reduce_sum | solution.py:45
  107.7 2.9 copy.47
  110.6 5.6 %copy.48 = f32[1,512,16,128]{1,2,3,0:T(8,128)} copy(f32[1,512,16,128]{3,2,1,0:T(8,128)} %bitcast.92) | data formatting | bytes 8388608 | tf_op jit(solution)/shard_map/reshape.112
  116.2 10.8 %fusion.67 = f32[1,512,16,128]{1,2,3,0:T(8,128)S(1)} fusion(f32[1,512,16,128]{1,2,3,0:T(8,128)} %copy.48), kind=kOutput, calls=%fused_computation.52.clone.1 | output fusion | flops 133169152 | bytes 8388608 | tf_op jit(solution)/shard_map/reduce-window.4
  127.0 0.0 copy-start.1
  127.0 1.9 copy-done.1
  128.9 0.1 reduce-window.20
  129.0 0.1 copy.49
  129.2 2.6 broadcast.100
  131.8 5.8 %copy.50 = f32[1,512,16,128]{3,2,1,0:T(8,128)} copy(f32[1,512,16,128]{1,2,3,0:T(8,128)} %copy-done.1) | data formatting | bytes 8388608 | tf_op jit(solution)/shard_map/reduce-window.4
  137.6 10.4 %fusion.68 = f32[1,512,128]{2,1,0:T(8,128)S(1)} fusion(f32[1,512,128]{2,1,0:T(8,128)S(1)} %get-tuple-element.245, bf16[2048,128]{1,0:T(8,128)(2,1)S(1)} %get-tuple-element.265, f32[64,8,16,128]{3,2,1,0:T(8,128)} %bitcast.93, f32[64,8,16,128]{3,2,1,0:T(8,128)} %bitcast.94, f32[512,2048]{1,0:T(8,128)} %fusion.64, f32[512]{0:T(512)S(1)} %bitcast.101, ...), kind=kOutput, calls=%fused_computation.16.clone.1 | convolution fusion | flops 294715392 | bytes 13651968 | tf_op jit(solution)/shard_map/while/body/grk,kgd->grd/dot_general | solution.py:42
  148.2 0.0 copy-start.2
  148.2 0.1 copy.23
  148.4 0.1 multiply_reduce_fusion
  148.5 0.0 copy-done.3
  148.5 0.1 fusion.38
  148.6 0.0 copy-done
  148.6 0.0 copy-start.4
  148.7 0.5 fusion.41
  149.1 0.0 copy-done.2
  149.2 0.1 add_dynamic-update-slice_fusion
  149.3 40.4 %all-reduce.1 = bf16[256,2048]{1,0:T(8,128)(2,1)} all-reduce(f32[256,2048]{1,0:T(8,128)S(1)} %add_dynamic-update-slice_fusion), channel_id=1, replica_groups=mesh['sp'=8,'tp'=4] {'tp'}, use_global_device_ids=true, to_apply=%region_6.7 | all-reduce | flops 524288 | bytes 3145728 | tf_op jit(solution)/shard_map/psum | solution.py:89
  189.7 1.5 fusion.29
  191.2 0.0 all-gather.3.cloned.1.call-done
  191.2 78.2 %all-gather.5.cloned.1.call-done = bf16[2048,2048]{1,0:T(8,128)(2,1)} async-done(((bf16[2048,256]{1,0:T(8,128)(2,1)}), bf16[2048,2048]{1,0:T(8,128)(2,1)}) %all-gather.5.cloned.1.call-update) | async-done | bytes 8388624 | tf_op jit(solution)/shard_map/all_gather | solution.py:102
  269.4 0.0 copy-done.4
  269.4 11.6 %convolution_convert_fusion = bf16[256,2048]{1,0:T(8,128)(2,1)} fusion(bf16[2048,2048]{1,0:T(8,128)(2,1)} %all-gather.5.cloned.1.call-done, bf16[2048,2048]{1,0:T(8,128)(2,1)} %all-gather.3.cloned.1.call-done, bf16[256,2048]{1,0:T(8,128)(2,1)} %all-reduce.1, f32[2048]{0:T(1024)S(1)} %copy-done.4, f32[256]{0:T(256)S(1)} %add_rsqrt_fusion.1), kind=kOutput, calls=%fused_computation.37 | convolution fusion | flops 4299161600 | bytes 18883584 | tf_op jit(solution)/shard_map/dot_general | solution.py:100
  281.1 0.0 reduce-scatter.2.cloned.1.call-update
  281.1 23.1 %reduce-scatter.2.cloned.1.call-done = bf16[256,512]{1,0:T(8,128)(2,1)} async-done(((bf16[256,2048]{1,0:T(8,128)(2,1)}), bf16[256,512]{1,0:T(8,128)(2,1)}) %reduce-scatter.2.cloned.1.call-update) | async-done | bytes 262160 | tf_op jit(solution)/shard_map/reduce_scatter | solution.py:105
  304.2 1.8 add_convert_fusion
  (11 shorter events, 0.1 us)
Async XLA Ops:
  6.5 142.1 %copy-start = (bf16[256,2048]{1,0:T(8,128)(2,1)S(1)}, bf16[256,2048]{1,0:T(8,128)(2,1)}, u32[]{:S(2)}) copy-start(bf16[256,2048]{1,0:T(8,128)(2,1)} %param.18) | copy-start | bytes 3145732
  6.5 184.7 %all-gather.3.cloned.1.call-start = ((), (), s32[]{:S(2)}) async-start(), calls=%async_computation.1 | async-start | bytes 9437184 | tf_op jit(solution)/shard_map/all_gather | solution.py:96
  7.3 262.1 %all-gather.5.cloned.1.call-start = ((), (), s32[]{:S(2)}) async-start(), calls=%async_computation.2 | async-start | bytes 9437184 | tf_op jit(solution)/shard_map/all_gather | solution.py:102
  8.0 296.2 %reduce-scatter.2.cloned.1.call-start = ((), (), s32[]{:S(2)}) async-start(), calls=%async_computation.3 | async-start | bytes 1310720 | tf_op jit(solution)/shard_map/reduce_scatter | solution.py:105
  99.9 48.6 %copy-start.3 = (f32[256]{0:T(256)S(1)}, f32[256]{0:T(256)}, u32[]{:S(2)}) copy-start(f32[256]{0:T(256)} %param.17) | copy-start | bytes 3076
  127.0 1.9 copy-start.1
  148.2 1.0 copy-start.2
  148.6 120.8 %copy-start.4 = (f32[2048]{0:T(1024)S(1)}, f32[2048]{0:T(1024)}, u32[]{:S(2)}) copy-start(f32[2048]{0:T(1024)} %param.19) | copy-start | bytes 24580
Sparse Core Ops, SparseCore 0:
  9.5 134.2 all-gather.2
  145.8 123.5 all-gather.4
  281.2 22.9 reduce-scatter.1
where the time goes:
time: 313 us
  blocking collectives  131 us (42%)
  waiting for transfers between devices  103 us (33%)
  matrix products  25.2 us (8%)
  local copies, waits for them, and re-layouts  20.1 us (6%)
  other arithmetic  19.6 us (6%)
  between operations  13.2 us (4%)
    all_gather x1, waiting for transfers between devices, body(): lax.all_gather(down_weight, 'sp', axis=1, tiled=True)  78.2 us
    psum x1, blocking collectives, body(): hidden_whole = lax.psum(partial_value, 'tp').astype(jnp.bfloat16)  40.4 us
    all_gather x1, blocking collectives, body(): lax.all_gather(key_rows, 'sp', axis=0, tiled=True)  35.3 us
    all_gather x1, blocking collectives, body(): lax.all_gather(value_rows, 'sp', axis=0, tiled=True)  33.5 us
    reduce_scatter x1, waiting for transfers between devices, body(): lax.psum_scatter(expanded.astype(jnp.bfloat16), 'tp', scatter_dimension=1...  23.1 us
    all_gather x1, blocking collectives, body(): lax.all_gather(break_shift, 'sp', axis=1, tiled=True)  22 us
    another operation x6, local copies, waits for them, and re-layouts  14.1 us
    dot_general x1, matrix products, body(): jnp.dot(activated, lax.all_gather(down_weight, 'sp', axis=1, tiled=True),...  11.6 us
  transfers between devices with their start and end apart: 3, of which 2 were waited for; matrix products, arithmetic and copies ran while one was open for 16% of the time, Pallas kernels for 0%

commit v1 on v0

--- a/solution.py
+++ b/solution.py
@@ -99,7 +99,7 @@
     activated = jnp.square(jax.nn.relu(lifted)).astype(jnp.bfloat16)
     expanded = jnp.dot(
         activated,
-        lax.all_gather(down_weight, "sp", axis=1, tiled=True),
+        jnp.concatenate(lax.all_gather(down_weight, "sp"), axis=1),
         preferred_element_type=jnp.float32,
     )
     mlp_total = lax.psum_scatter(

time: 313 us -> 313 us (level)
  waiting for transfers between devices: 103 us -> 90.6 us
  local copies, waits for them, and re-layouts: 20.1 us -> 31.9 us
    all_gather x1, waiting for transfers between devices: 78.2 us -> 0.02 us  [body(): lax.all_gather(down_weight, 'sp')]
    all_gather x1, waiting for transfers between devices: 0.02 us -> 66 us  [body(): lax.all_gather(up_weight, 'sp', axis=0, tiled=True)]
    reshape x0 -> x1, local copies, waits for them, and re-layouts: none -> 11.8 us  [body(): jnp.concatenate(lax.all_gather(down_weight, 'sp'), axis=1)]
  transfers between devices with their start and end apart: 3 -> 3, of which waited for: 2 -> 2; matrix products, arithmetic and copies ran while one was open for 16% -> 20% of each run, Pallas kernels for 0% -> 0%
where the time goes in v1:
time: 313 us; the launch traced here: 312 us
  blocking collectives  131 us (42%)
  waiting for transfers between devices  90.6 us (29%)
  local copies, waits for them, and re-layouts  31.9 us (10%)
  matrix products  24.9 us (8%)
  other arithmetic  19.6 us (6%)
  between operations  13.2 us (4%)
    all_gather x1, waiting for transfers between devices, body(): lax.all_gather(up_weight, 'sp', axis=0, tiled=True)  66 us
    psum x1, blocking collectives, body(): hidden_whole = lax.psum(partial_value, 'tp').astype(jnp.bfloat16)  40.4 us
    all_gather x1, blocking collectives, body(): lax.all_gather(key_rows, 'sp', axis=0, tiled=True)  35.3 us
    all_gather x1, blocking collectives, body(): lax.all_gather(value_rows, 'sp', axis=0, tiled=True)  33.5 us
    reduce_scatter x1, waiting for transfers between devices, body(): lax.psum_scatter(expanded.astype(jnp.bfloat16), 'tp', scatter_dimension=1...  23.1 us
    all_gather x1, blocking collectives, body(): lax.all_gather(break_shift, 'sp', axis=1, tiled=True)  22 us
    another operation x6, local copies, waits for them, and re-layouts  14.1 us
    reshape x1, local copies, waits for them, and re-layouts, body(): jnp.concatenate(lax.all_gather(down_weight, 'sp'), axis=1)  11.8 us
  transfers between devices with their start and end apart: 3, of which 2 were waited for; matrix products, arithmetic and copies ran while one was open for 20% of the time, Pallas kernels for 0%

profile of v1, /device:TPU:0, one launch (start us, length us, event | category | flops | bytes accessed | tf_op | source)
XLA Modules:
  0.0 311.8 jit_solution(12984909615525953081)
XLA Ops:
  6.5 0.0 copy-start
  6.5 0.0 all-gather.6.cloned.1.call-start
  6.5 0.7 all-gather.6.cloned.1.call-update
  7.3 0.0 all-gather.4.cloned.1.call-start
  7.3 0.7 all-gather.4.cloned.1.call-update
  8.0 0.0 reduce-scatter.2.cloned.1.call-start
  8.1 35.3 %all_gather.18 = bf16[2048,128]{1,0:T(8,128)(2,1)S(1)} all-gather(bf16[256,128]{1,0:T(8,128)(2,1)} %param.14), channel_id=1, replica_groups=mesh['sp'=8,'tp'=4] {'sp'}, dimensions={0}, use_global_device_ids=true | all-gather | bytes 589824 | tf_op jit(solution)/shard_map/all_gather | solution.py:71
  43.4 33.5 %all_gather.20 = bf16[2048,128]{1,0:T(8,128)(2,1)S(1)} all-gather(bf16[256,128]{1,0:T(8,128)(2,1)} %param.15), channel_id=1, replica_groups=mesh['sp'=8,'tp'=4] {'sp'}, dimensions={0}, use_global_device_ids=true | all-gather | bytes 589824 | tf_op jit(solution)/shard_map/all_gather | solution.py:72
  76.9 0.9 reshape.150
  77.9 22.0 %all_gather.19 = bf16[1,2048]{1,0:T(2,128)(2,1)S(1)} all-gather(bf16[1,256]{1,0:T(2,128)(2,1)} %param.16), channel_id=1, replica_groups=mesh['sp'=8,'tp'=4] {'sp'}, dimensions={1}, use_global_device_ids=true | all-gather | bytes 4608 | tf_op jit(solution)/shard_map/all_gather | solution.py:73
  99.9 0.0 copy-start.4
  99.9 48.2 %while.15 = (s32[]{:T(128)}, f32[1,512,128]{2,1,0:T(8,128)S(1)}, f32[1,512]{1,0:T(1,128)S(1)}, s32[]{:T(128)}, s32[]{:T(128)}, /*index=5*/bf16[1,512,128]{2,1,0:...) while((s32[]{:T(128)}, f32[1,512,128]{2,1,0:T(8,128)S(1)}, ...), condition=%wide.region_4.5_spmd.clone, body=%wide.region_0.4_spmd.clone.sunk | while | flops 709041152 | bytes 81762496 | solution.py:51
  100.0 2.6 fusion.64
  102.6 5.0 %fusion.66 = (f32[512]{0:T(512)S(1)}, f32[64,8,16,128]{3,1,2,0:T(8,128)S(1)}) fusion(f32[2048]{0:T(1024)S(1)} %bitcast.104, f32[512,2048]{1,0:T(8,128)} %fusion.64, s32[512]{0:T(512)S(1)} %fusion.65, s32[2048]{0:T(1024)S(1)} %iota_add_fusion.2), kind=kLoop, calls=%fused_computation.30.clone.1 | loop fusion | flops 12582400 | bytes 8409088 | tf_op jit(solution)/shard_map/while/body/reduce_sum | solution.py:45
  107.7 2.9 copy.48
  110.6 5.6 %copy.49 = f32[1,512,16,128]{1,2,3,0:T(8,128)} copy(f32[1,512,16,128]{3,2,1,0:T(8,128)} %bitcast.96) | data formatting | bytes 8388608 | tf_op jit(solution)/shard_map/reshape.114
  116.2 10.8 %fusion.67 = f32[1,512,16,128]{1,2,3,0:T(8,128)S(1)} fusion(f32[1,512,16,128]{1,2,3,0:T(8,128)} %copy.49), kind=kOutput, calls=%fused_computation.52.clone.1 | output fusion | flops 133169152 | bytes 8388608 | tf_op jit(solution)/shard_map/reduce-window.4
  127.0 0.0 copy-start.1
  127.0 1.9 copy-done.1
  128.9 0.1 reduce-window.20
  129.0 0.1 copy.50
  129.2 2.6 broadcast.100
  131.8 5.8 %copy.51 = f32[1,512,16,128]{3,2,1,0:T(8,128)} copy(f32[1,512,16,128]{1,2,3,0:T(8,128)} %copy-done.1) | data formatting | bytes 8388608 | tf_op jit(solution)/shard_map/reduce-window.4
  137.6 10.4 %fusion.68 = f32[1,512,128]{2,1,0:T(8,128)S(1)} fusion(f32[1,512,128]{2,1,0:T(8,128)S(1)} %get-tuple-element.245, bf16[2048,128]{1,0:T(8,128)(2,1)S(1)} %get-tuple-element.265, f32[64,8,16,128]{3,2,1,0:T(8,128)} %bitcast.97, f32[64,8,16,128]{3,2,1,0:T(8,128)} %bitcast.98, f32[512,2048]{1,0:T(8,128)} %fusion.64, f32[512]{0:T(512)S(1)} %bitcast.107, ...), kind=kOutput, calls=%fused_computation.16.clone.1 | convolution fusion | flops 294715392 | bytes 13651968 | tf_op jit(solution)/shard_map/while/body/grk,kgd->grd/dot_general | solution.py:42
  148.2 0.0 copy-start.3
  148.2 0.1 copy.23
  148.4 0.1 multiply_reduce_fusion
  148.5 0.0 copy-done.4
  148.5 0.1 fusion.38
  148.6 0.0 copy-done
  148.6 0.5 fusion.41
  149.1 0.1 copy-done.3
  149.2 0.1 add_dynamic-update-slice_fusion
  149.3 40.4 %all-reduce.1 = bf16[256,2048]{1,0:T(8,128)(2,1)} all-reduce(f32[256,2048]{1,0:T(8,128)S(1)} %add_dynamic-update-slice_fusion), channel_id=1, replica_groups=mesh['sp'=8,'tp'=4] {'tp'}, use_global_device_ids=true, to_apply=%region_6.7 | all-reduce | flops 524288 | bytes 3145728 | tf_op jit(solution)/shard_map/psum | solution.py:89
  189.7 1.5 fusion.29
  191.2 0.0 all-gather.6.cloned.1.call-done
  191.2 0.0 copy-start.2
  191.2 0.0 copy-start.5
  191.2 11.8 %copy.24 = bf16[2048,8,256]{0,2,1:T(8,128)(2,1)} copy(bf16[2048,8,256]{2,0,1:T(8,128)(2,1)} %bitcast.99) | data formatting | bytes 16777216 | tf_op jit(solution)/shard_map/reshape | solution.py:102
  203.0 66.0 %all-gather.4.cloned.1.call-done = bf16[2048,2048]{1,0:T(8,128)(2,1)} async-done(((bf16[256,2048]{1,0:T(8,128)(2,1)}), bf16[2048,2048]{1,0:T(8,128)(2,1)}) %all-gather.4.cloned.1.call-update) | async-done | bytes 8388624 | tf_op jit(solution)/shard_map/all_gather | solution.py:96
  269.0 0.0 copy-done.2
  269.0 0.0 copy-done.5
  269.0 11.4 %convolution_convert_fusion = bf16[256,2048]{1,0:T(8,128)(2,1)} fusion(bf16[2048,2048]{0,1:T(8,128)(2,1)} %bitcast.100, bf16[2048,2048]{1,0:T(8,128)(2,1)} %all-gather.4.cloned.1.call-done, bf16[256,2048]{1,0:T(8,128)(2,1)S(1)} %copy-done.2, f32[2048]{0:T(1024)S(1)} %copy-done.5, f32[256]{0:T(256)S(1)} %add_rsqrt_fusion.1), kind=kOutput, calls=%fused_computation.37 | convolution fusion | flops 4299161600 | bytes 18883584 | tf_op jit(solution)/shard_map/dot_general | solution.py:100
  280.4 0.0 reduce-scatter.2.cloned.1.call-update
  280.4 23.1 %reduce-scatter.2.cloned.1.call-done = bf16[256,512]{1,0:T(8,128)(2,1)} async-done(((bf16[256,2048]{1,0:T(8,128)(2,1)}), bf16[256,512]{1,0:T(8,128)(2,1)}) %reduce-scatter.2.cloned.1.call-update) | async-done | bytes 262160 | tf_op jit(solution)/shard_map/reduce_scatter | solution.py:105
  303.6 1.7 add_convert_fusion
  (11 shorter events, 0.1 us)
Async XLA Ops:
  6.5 142.1 %copy-start = (bf16[256,2048]{1,0:T(8,128)(2,1)S(1)}, bf16[256,2048]{1,0:T(8,128)(2,1)}, u32[]{:S(2)}) copy-start(bf16[256,2048]{1,0:T(8,128)(2,1)} %param.18) | copy-start | bytes 3145732
  6.5 184.7 %all-gather.6.cloned.1.call-start = ((), (), s32[]{:S(2)}) async-start(), calls=%async_computation.3 | async-start | bytes 9437184 | tf_op jit(solution)/shard_map/all_gather | solution.py:102
  7.3 261.8 %all-gather.4.cloned.1.call-start = ((), (), s32[]{:S(2)}) async-start(), calls=%async_computation.1 | async-start | bytes 9437184 | tf_op jit(solution)/shard_map/all_gather | solution.py:96
  8.0 295.6 %reduce-scatter.2.cloned.1.call-start = ((), (), s32[]{:S(2)}) async-start(), calls=%async_computation.2 | async-start | bytes 1310720 | tf_op jit(solution)/shard_map/reduce_scatter | solution.py:105
  99.9 48.6 %copy-start.4 = (f32[256]{0:T(256)S(1)}, f32[256]{0:T(256)}, u32[]{:S(2)}) copy-start(f32[256]{0:T(256)} %param.17) | copy-start | bytes 3076
  127.0 1.9 copy-start.1
  148.2 1.0 copy-start.3
  191.2 77.8 %copy-start.2 = (bf16[256,2048]{1,0:T(8,128)(2,1)S(1)}, bf16[256,2048]{1,0:T(8,128)(2,1)}, u32[]{:S(2)}) copy-start(bf16[256,2048]{1,0:T(8,128)(2,1)} %all-reduce.1) | copy-start | bytes 3145732
  191.2 77.8 %copy-start.5 = (f32[2048]{0:T(1024)S(1)}, f32[2048]{0:T(1024)}, u32[]{:S(2)}) copy-start(f32[2048]{0:T(1024)} %param.19) | copy-start | bytes 24580
Sparse Core Ops, SparseCore 0:
  9.5 134.2 all-gather.5
  145.8 123.1 all-gather.3
  280.6 22.9 reduce-scatter.1
